TPU v7x, 32 devices: a whole 2x2x4 slice. The times are simulated.
32 devices in a mesh: rep: 4 (over z), fs: 4 (over y, x), tp: 2 (over core).
Axes of the slice: x: 2, y: 2, z: 4, core: 2. Of those that a mesh axis runs over, the one named last changes fastest.
Arguments:
- tokens: bfloat16 [16, 768, 2048], P(('rep', 'fs')), may hold values from -6 to 6
- norm_gain: float32 [2048], replicated, may hold values from 0.1 to 1.9
- outer_weight: bfloat16 [2048, 2048], P('fs', 'tp'), may hold values from -0.125 to 0.125
- inner_weight: bfloat16 [2048, 2048], P('fs', 'tp'), may hold values from -0.125 to 0.125
- value_weight: bfloat16 [2048, 2048], P('fs', 'tp'), may hold values from -0.125 to 0.125
- conv_taps: float32 [3, 2048], replicated, may hold values from -3.5 to 3.5
- out_weight: bfloat16 [2048, 2048], P('fs', 'tp'), may hold values from -0.125 to 0.125
Outputs:
- mixed: bfloat16 [16, 768, 2048], P(('rep', 'fs'), None, 'tp')
All inputs are finite; a program needn't handle non-finite values.
Results may differ from a plain program's by a relative error of at most 0.014.
Values may be sent and summed in bfloat16 or wider, within the bound.
A program may use at most 64 MiB of HBM per device.

v0:
```python
import functools

import jax
import jax.numpy as jnp
from jax import lax
from jax.experimental import pallas as pl
from jax.experimental.pallas import tpu as pltpu
from jax.sharding import PartitionSpec as P

MESH = pl.DeviceIdType.MESH
F32 = jnp.float32
BF16 = jnp.bfloat16


def plain(tokens, norm_gain, outer_weight, inner_weight, value_weight, conv_taps, out_weight):
    batch, seq_len, width = tokens.shape
    xf = tokens.astype(F32)
    scale = lax.rsqrt(jnp.mean(xf * xf, axis=-1, keepdims=True) + 1e-06)
    normed = (xf * scale * norm_gain).astype(BF16).reshape(batch * seq_len, width)
    columns = outer_weight.shape[1]

    def project(weight):
        full = lax.all_gather(weight, "fs", axis=0, tiled=True)
        return jnp.dot(normed, full, preferred_element_type=F32).astype(BF16).astype(F32)

    outer, inner, value = project(outer_weight), project(inner_weight), project(value_weight)
    product = (inner * value).reshape(batch, seq_len, columns)
    offset = lax.axis_index("tp") * columns
    taps = lax.dynamic_slice_in_dim(conv_taps, offset, columns, 1)
    count = conv_taps.shape[0]
    padded = jnp.pad(product, ((0, 0), (count - 1, 0), (0, 0)))
    convolved = jnp.zeros((batch, seq_len, columns), F32)
    for k in range(count):
        convolved = convolved + taps[k] * padded[:, k : k + seq_len, :]
    gated = (outer * convolved.reshape(batch * seq_len, columns)).astype(BF16)
    everything = lax.all_gather(gated, "tp", axis=1, tiled=True)
    full = lax.all_gather(out_weight, "fs", axis=0, tiled=True)
    result = jnp.dot(everything, full, preferred_element_type=F32)
    return result.astype(BF16).reshape(batch, seq_len, columns)


def kernel(
    tok_hbm, gain_ref, outer_hbm, inner_hbm, value_hbm, taps_ref, outw_hbm, out_ref,
    tok, nm, wts, outw, acc, prod, gat, mine, osum, send_sems, recv_sems, local_sems,
):
    rep, fs, tp = lax.axis_index("rep"), lax.axis_index("fs"), lax.axis_index("tp")
    seq, width = tok_hbm.shape
    rows, cols = outer_hbm.shape
    half = cols // 2
    part = half // PARTS
    hrows = rows // 2
    count = taps_ref.shape[0]
    par = lax.rem(rep, 2)
    fx = fs + 1 - 2 * lax.rem(fs, 2)
    fy = lax.rem(fs + 2, 4)
    fd = 3 - fs
    shard = (fs, fx, fy, fd)
    to_x, to_y = (rep, fx, tp), (rep, fy, tp)
    to_z, to_t = (rep + 1 - 2 * par, fs, tp), (rep, fs, 1 - tp)
    used = [0]

    def remote(src, dst, device):
        k = used[0]
        used[0] += 1
        return pltpu.make_async_remote_copy(
            src_ref=src, dst_ref=dst, send_sem=send_sems.at[k], recv_sem=recv_sems.at[k],
            device_id=device, device_id_type=MESH,
        )

    barrier = pltpu.get_barrier_semaphore()
    for peer in (to_x, to_y, to_z, to_t):
        pl.semaphore_signal(barrier, inc=1, device_id=peer, device_id_type=MESH)

    hbm = (inner_hbm, value_hbm, outer_hbm)
    pieces = [(c, w) for c in range(PARTS) for w in range(3)]

    def mycols(c):
        return pl.ds(pl.multiple_of(par * half + c * part, part), part)

    tok_load = pltpu.make_async_copy(tok_hbm, tok.at[0], local_sems.at[0])
    ow_load = pltpu.make_async_copy(outw_hbm, outw.at[0], local_sems.at[1])
    w_load = {
        (c, w): pltpu.make_async_copy(hbm[w].at[:, mycols(c)], wts.at[c, w, 0], local_sems.at[2 + i])
        for i, (c, w) in enumerate(pieces)
    }
    tok_load.start()
    for p in pieces:
        w_load[p].start()
    ow_load.start()

    chunks = 2
    crow = seq // 2 // chunks
    trow = [pl.ds(pl.multiple_of(tp * (seq // 2) + c * crow, 8), crow) for c in range(chunks)]
    tok_z = [remote(tok_hbm.at[r], tok.at[1, r], to_z) for r in trow]
    tok_t = [remote(tok.at[1, r], tok.at[1, r], to_t) for r in trow]
    low, high = pl.ds(0, hrows), pl.ds(hrows, hrows)
    w_x, w_y, d_x, d_y = {}, {}, {}, {}
    for c, w in pieces:
        src = hbm[w].at[:, mycols(c)]
        w_x[c, w] = remote(src, wts.at[c, w, 1], to_x)
        w_y[c, w] = remote(src, wts.at[c, w, 2], to_y)
        d_x[c, w] = remote(wts.at[c, w, 2, low], wts.at[c, w, 3, low], to_x)
        d_y[c, w] = remote(wts.at[c, w, 1, high], wts.at[c, w, 3, high], to_y)
    one = pl.ds(pl.multiple_of(par * hrows, hrows), hrows)
    two = pl.ds(pl.multiple_of((1 - par) * hrows, hrows), hrows)
    o_y = remote(outw_hbm.at[one], outw.at[2, one], to_y)
    o_x = remote(outw_hbm.at[two], outw.at[1, two], to_x)
    oz_y = remote(outw.at[2, one], outw.at[2, one], to_z)
    oz_x = remote(outw.at[1, two], outw.at[1, two], to_z)
    od_x = remote(outw.at[2, one], outw.at[3, one], to_x)
    od_y = remote(outw.at[1, two], outw.at[3, two], to_y)
    group, other = tp * 2 + par, tp * 2 + 1 - par
    peer_group, peer_other = (1 - tp) * 2 + par, (1 - tp) * 2 + 1 - par
    g_z = [remote(mine.at[c], gat.at[group, c], to_z) for c in range(PARTS)]
    g_t = [remote(gat.at[group, c], gat.at[group, c], to_t) for c in range(PARTS)]
    g_f = [remote(gat.at[other, c], gat.at[other, c], to_t) for c in range(PARTS)]

    pl.semaphore_wait(barrier, 4)
    for r in range(chunks):
        tok_z[r].start()
    for w in range(3):
        w_x[0, w].start()
        w_y[0, w].start()
    o_y.start()
    o_x.start()

    tile = 128

    def norm(s):
        @pl.loop(0, seq // tile)
        def _(b):
            r = pl.multiple_of(b * tile, tile)
            xf = tok[s, pl.ds(r, tile), :].astype(F32)
            scale = lax.rsqrt(jnp.mean(xf * xf, axis=-1, keepdims=True) + 1e-06)
            y = (xf * scale * gain_ref[...]).astype(BF16)
            for j in range(4):
                nm[j, pl.ds(s * seq + r, tile), :] = y[:, j * rows : (j + 1) * rows]

    mt = 256

    def project(c, w, slots, start, length, fresh):
        @pl.loop(0, length // mt)
        def _(b):
            r = pl.ds(pl.multiple_of(start + b * mt, mt), mt)
            total = None
            for s in slots:
                d = jnp.dot(nm[shard[s], r, :], wts[c, w, s], preferred_element_type=F32)
                total = d if total is None else total + d
            if fresh:
                acc[c, w, r, :] = total
            else:
                acc[c, w, r, :] += total

    prod[0:8, :] = jnp.zeros((8, part), F32)

    def gate(c, s, store):
        tcols = pl.ds(pl.multiple_of(tp * cols + par * half + c * part, part), part)

        @pl.loop(0, seq // tile)
        def _(b):
            r = pl.multiple_of(b * tile, tile)
            a = pl.ds(s * seq + r, tile)
            inner = acc[c, 0, a, :].astype(BF16).astype(F32)
            value = acc[c, 1, a, :].astype(BF16).astype(F32)
            outer = acc[c, 2, a, :].astype(BF16).astype(F32)
            prod[pl.ds(r + 8, tile), :] = inner * value
            window = prod[pl.ds(r, tile + 8), :]
            conv = jnp.zeros((tile, part), F32)
            for k in range(count):
                lo = 8 - (count - 1) + k
                conv = conv + taps_ref[k : k + 1, tcols] * window[lo : lo + tile, :]
            store(pl.ds(r, tile), (outer * conv).astype(BF16))

    def keep_partner(c):
        def store(r, x):
            mine[c, r, :] = x
        return store

    def keep_own(c):
        def store(r, x):
            gat[group, c, r, :] = x
        return store

    tok_load.wait()
    norm(0)
    for w in range(3):
        w_load[0, w].wait()
        w_y[0, w].wait_recv()
        d_x[0, w].start()
        w_x[0, w].wait_recv()
        d_y[0, w].start()
        if w == 2:
            for v in range(3):
                w_x[1, v].start()
                w_y[1, v].start()
        project(0, w, (0, 1, 2), 0, seq, True)
    tok_z[0].wait_recv()
    tok_t[0].start()
    for w in range(3):
        w_load[1, w].wait()
        project(1, w, (0,), 0, seq, True)
    o_y.wait_recv()
    oz_y.start()
    o_x.wait_recv()
    oz_x.start()
    tok_z[1].wait_recv()
    tok_t[1].start()
    for w in range(3):
        d_x[0, w].wait_recv()
        d_y[0, w].wait_recv()
        project(0, w, (3,), 0, seq, False)
    gate(0, 0, keep_own(0))
    tok_t[0].wait_recv()
    tok_t[1].wait_recv()
    norm(1)
    g_t[0].start()
    for w in range(3):
        project(0, w, (0, 1, 2, 3), seq, seq, True)
    w_y[1, 0].wait_recv()
    d_x[1, 0].start()
    w_x[1, 0].wait_recv()
    d_y[1, 0].start()
    gate(0, 1, keep_partner(0))
    for w in range(3):
        if w > 0:
            w_y[1, w].wait_recv()
            d_x[1, w].start()
            w_x[1, w].wait_recv()
            d_y[1, w].start()
        else:
            project(1, w, (1, 2), 0, seq, False)
            g_z[0].start()
        if w == 2:
            od_x.start()
            od_y.start()
        if w > 0:
            project(1, w, (1, 2), 0, seq, False)
        project(1, w, (0, 1, 2), seq, seq, True)
    for w in range(3):
        d_x[1, w].wait_recv()
        d_y[1, w].wait_recv()
        project(1, w, (3,), seq, seq, False)
        if w < 2:
            project(1, w, (3,), 0, seq, False)
    gate(1, 1, keep_partner(1))
    project(1, 2, (3,), 0, seq, False)
    g_z[1].start()
    gate(1, 0, keep_own(1))
    g_z[0].wait_recv()
    g_f[0].start()
    g_t[0].wait_recv()
    oz_y.wait_recv()
    oz_x.wait_recv()
    ow_load.wait()
    g_t[1].start()
    g_f[0].wait_recv()

    def slot(g):
        return lax.rem(g + fs, 2) + 2 * lax.rem(g // 2 + fs // 2, 2)

    def mix(terms, first, last):
        @pl.loop(0, seq // mt)
        def _(b):
            r = pl.ds(pl.multiple_of(b * mt, mt), mt)
            total = None
            for g, s, c in terms:
                d = jnp.dot(
                    gat[g, c, r, :], outw[s, c * part : (c + 1) * part, :],
                    preferred_element_type=F32,
                )
                total = d if total is None else total + d
            if not first:
                total = total + osum[r, :]
            if last:
                out_ref[r, :] = total.astype(BF16)
            else:
                osum[r, :] = total

    mix([(shard[s], s, 0) for s in range(3)], True, False)
    od_x.wait_recv()
    od_y.wait_recv()
    g_t[1].wait_recv()
    mix([(fd, 3, 0), (group, slot(group), 1), (peer_group, slot(peer_group), 1)], False, False)
    g_z[1].wait_recv()
    g_f[1].start()
    mix([(other, slot(other), 1)], False, False)
    g_f[1].wait_recv()
    mix([(peer_other, slot(peer_other), 1)], False, True)

    sent = tok_z + tok_t + [o_x, o_y, oz_x, oz_y, od_x, od_y] + g_z + g_t + g_f
    for p in pieces:
        sent += [w_x[p], w_y[p], d_x[p], d_y[p]]
    for c in sent:
        c.wait_send()


PARTS = 2
COPIES = 40


def paired(tokens, norm_gain, outer_weight, inner_weight, value_weight, conv_taps, out_weight):
    _, seq, width = tokens.shape
    rows, cols = outer_weight.shape
    half = cols // 2
    anyspace = pl.BlockSpec(memory_space=pltpu.HBM)
    vmem = pl.BlockSpec(memory_space=pltpu.VMEM)
    out = pl.pallas_call(
        kernel,
        out_shape=pltpu.VMEM((seq, cols), BF16),
        in_specs=[anyspace, vmem, anyspace, anyspace, anyspace, vmem, anyspace],
        out_specs=vmem,
        scratch_shapes=[
            pltpu.VMEM((2, seq, width), BF16),
            pltpu.VMEM((4, 2 * seq, rows), BF16),
            pltpu.VMEM((PARTS, 3, 4, rows, half // PARTS), BF16),
            pltpu.VMEM((4, rows, cols), BF16),
            pltpu.VMEM((PARTS, 3, 2 * seq, half // PARTS), F32),
            pltpu.VMEM((seq + 8, half // PARTS), F32),
            pltpu.VMEM((4, PARTS, seq, half // PARTS), BF16),
            pltpu.VMEM((PARTS, seq, half // PARTS), BF16),
            pltpu.VMEM((seq, cols), F32),
            pltpu.SemaphoreType.DMA((COPIES,)),
            pltpu.SemaphoreType.DMA((COPIES,)),
            pltpu.SemaphoreType.DMA((2 + 3 * PARTS,)),
        ],
        compiler_params=pltpu.CompilerParams(
            collective_id=0, has_side_effects=True, vmem_limit_bytes=58 * 1024 * 1024
        ),
        name="mixer",
    )(
        tokens.reshape(seq, width), norm_gain.reshape(1, width), outer_weight, inner_weight,
        value_weight, conv_taps, out_weight,
    )
    return out.reshape(1, seq, cols)


def solution(mesh):
    shape = dict(mesh.shape)

    def local(tokens, *rest):
        rows, cols = rest[1].shape
        fits = (
            shape["fs"] == 4 and shape["tp"] == 2 and shape["rep"] % 2 == 0
            and tokens.shape[0] == 1 and tokens.shape[1] % 256 == 0
            and rows % 256 == 0 and cols == 2 * rows and rest[4].shape[0] <= 9
        )
        return (paired if fits else plain)(tokens, *rest)

    in_specs = (
        P(("rep", "fs"), None, None),
        P(),
        P("fs", "tp"),
        P("fs", "tp"),
        P("fs", "tp"),
        P(),
        P("fs", "tp"),
    )
    out_specs = P(("rep", "fs"), None, "tp")
    return jax.shard_map(local, mesh=mesh, in_specs=in_specs, out_specs=out_specs, check_vma=False)
```

profile of v0, /device:TPU:9, one launch (start us, length us, event | category | flops | bytes accessed | tf_op | source)
XLA Modules:
  0.0 84.1 jit_solution(2563503430617781477)
XLA Ops:
  0.0 82.9 %mixer.1 = bf16[768,1024]{1,0:T(8,128)(2,1)S(1)} custom-call(bf16[768,2048]{1,0:T(8,128)(2,1)} %bitcast.4, f32[1,2048]{1,0:T(1,128)} %bitcast.5, bf16[512,1024]{1,0:T(8,128)(2,1)} %outer_hbm.1, bf16[512,1024]{1,0:T(8,128)(2,1)} %inner_hbm.1, bf16[512,1024]{1,0:T(8,128)(2,1)} %value_hbm.1, f32[3,2048]{1,0:T(4,128)} %taps_ref.1, bf16[512,1024]{1,0:T(8,128)(2,1)} %outw_hbm.1), custom_call_target="tpu_custom_call" | custom-call | tf_op jit(solution)/shard_map/mixer/pallas_call | solution.py:307
  82.9 1.1 %copy.9 = bf16[1,768,1024]{2,1,0:T(8,128)(2,1)} copy(bf16[1,768,1024]{2,1,0:T(8,128)(2,1)S(1)} %bitcast.3) | data formatting | bytes 3145728
where the time goes:
time: 85.2 us; the launch traced here: 84.1 us
  Pallas kernels  82.9 us (97%)
  local copies, waits for them, and re-layouts  1.15 us (1%)
    pallas_call x1, Pallas kernels, paired(): pl.pallas_call(kernel, out_shape=pltpu.VMEM((seq, cols), BF16), in_specs=...  82.9 us

commit v1 on v0

v1 whole, which is shorter than its diff:
```python
import jax
import jax.numpy as jnp
from jax import lax
from jax.experimental import pallas as pl
from jax.experimental.pallas import tpu as pltpu
from jax.sharding import PartitionSpec as P

MESH = pl.DeviceIdType.MESH
F32 = jnp.float32
BF16 = jnp.bfloat16


def plain(tokens, norm_gain, outer_weight, inner_weight, value_weight, conv_taps, out_weight):
    batch, seq_len, width = tokens.shape
    xf = tokens.astype(F32)
    scale = lax.rsqrt(jnp.mean(xf * xf, axis=-1, keepdims=True) + 1e-06)
    normed = (xf * scale * norm_gain).astype(BF16).reshape(batch * seq_len, width)
    columns = outer_weight.shape[1]

    def project(weight):
        full = lax.all_gather(weight, "fs", axis=0, tiled=True)
        return jnp.dot(normed, full, preferred_element_type=F32).astype(BF16).astype(F32)

    outer, inner, value = project(outer_weight), project(inner_weight), project(value_weight)
    product = (inner * value).reshape(batch, seq_len, columns)
    offset = lax.axis_index("tp") * columns
    taps = lax.dynamic_slice_in_dim(conv_taps, offset, columns, 1)
    count = conv_taps.shape[0]
    padded = jnp.pad(product, ((0, 0), (count - 1, 0), (0, 0)))
    convolved = jnp.zeros((batch, seq_len, columns), F32)
    for k in range(count):
        convolved = convolved + taps[k] * padded[:, k : k + seq_len, :]
    gated = (outer * convolved.reshape(batch * seq_len, columns)).astype(BF16)
    everything = lax.all_gather(gated, "tp", axis=1, tiled=True)
    full = lax.all_gather(out_weight, "fs", axis=0, tiled=True)
    result = jnp.dot(everything, full, preferred_element_type=F32)
    return result.astype(BF16).reshape(batch, seq_len, columns)


PARTS = 4
PAD = 16
COPIES = 112


def kernel(
    tok_hbm, gain_ref, outer_hbm, inner_hbm, value_hbm, taps_ref, outw_hbm, out_ref,
    tok, nm, wts, outw, proj, gat, mine, osum, send_sems, recv_sems, local_sems,
):
    rep, fs, tp = lax.axis_index("rep"), lax.axis_index("fs"), lax.axis_index("tp")
    seq, width = tok_hbm.shape
    rows, cols = outer_hbm.shape
    part = cols // PARTS
    hseq = seq // 2
    hrows = rows // 2
    qrows = rows // 4
    count = taps_ref.shape[0]
    m = rep // 2
    inner_chip = lax.rem(rep, 2) + m - 2 * lax.rem(rep, 2) * m
    fx = fs + 1 - 2 * lax.rem(fs, 2)
    fy = lax.rem(fs + 2, 4)
    fd = 3 - fs
    fp = fy + m * (fx - fy)
    fq = fx + m * (fy - fx)
    to_x, to_y, to_p, to_q = (rep, fx, tp), (rep, fy, tp), (rep, fp, tp), (rep, fq, tp)
    to_z, to_t = (rep + 1 - 2 * lax.rem(rep, 2), fs, tp), (rep, fs, 1 - tp)
    to_m = (3 - rep, fs, tp)
    keys = {}

    barrier = pltpu.get_barrier_semaphore()
    for peer in (to_x, to_y, to_z, to_t):
        pl.semaphore_signal(barrier, inc=1, device_id=peer, device_id_type=MESH)

    hbm = (inner_hbm, value_hbm, outer_hbm)
    tok_load = pltpu.make_async_copy(tok_hbm, tok.at[0], local_sems.at[0])
    tok_load.start()

    def al(x, n):
        return pl.multiple_of(x, n)

    tile = 128

    def norm(s, h, halves):
        @pl.loop(0, halves * hseq // tile)
        def _(b):
            r = al(h * hseq + b * tile, tile)
            xf = tok[s, pl.ds(r, tile), :].astype(F32)
            scale = lax.rsqrt(jnp.mean(xf * xf, axis=-1, keepdims=True) + 1e-06)
            nm[pl.ds(al(s * seq + r, tile), tile), :] = (xf * scale * gain_ref[...]).astype(BF16)

    zeros = jnp.zeros((PAD, part), BF16)
    for c in range(PARTS - 1):
        for w in range(2):
            for s in range(2):
                proj[w, c, s, 0:PAD, :] = zeros

    def project(units, blocks):
        b0, nb = blocks[0], len(blocks)
        u0, nu = units[0], len(units)

        @pl.loop(0, nu * nb)
        def _(i):
            u = u0 + i // nb
            b = b0 + lax.rem(i, nb)
            s, h = b // 2, lax.rem(b, 2)
            d = jnp.dot(nm[pl.ds(al(b * hseq, 128), hseq), :], wts[u], preferred_element_type=F32)
            proj[lax.rem(u, 3), u // 3, s, pl.ds(al(PAD + h * hseq, PAD), hseq), :] = d.astype(BF16)

    def gate(c, first, s, h, halves, store):
        tcols = pl.ds(al(tp * cols + first + c * part, 128), part)

        @pl.loop(0, halves * hseq // tile)
        def _(b):
            r = al(h * hseq + b * tile, tile)
            inner = proj[0, c, s, pl.ds(r, tile + PAD), :].astype(F32)
            value = proj[1, c, s, pl.ds(r, tile + PAD), :].astype(F32)
            outer = proj[2, c, s, pl.ds(al(r + PAD, PAD), tile), :].astype(F32)
            window = inner * value
            conv = jnp.zeros((tile, part), F32)
            for k in range(count):
                lo = PAD - (count - 1) + k
                conv = conv + taps_ref[k : k + 1, tcols] * window[lo : lo + tile, :]
            store(pl.ds(r, tile), (outer * conv).astype(BF16))

    def mix(tile_rows, b0, nb, terms, first, last):
        @pl.loop(b0, b0 + nb)
        def _(b):
            r = pl.ds(al(b * tile_rows, tile_rows), tile_rows)
            total = None
            for k, n in terms:
                d = jnp.dot(gat[r, pl.ds(k, n)], outw[pl.ds(k, n), :], preferred_element_type=F32)
                total = d if total is None else total + d
            if not first:
                total = total + osum[r, :]
            if last:
                out_ref[r, :] = total.astype(BF16)
            else:
                osum[r, :] = total

    def program(inside):
        sent = []

        def index(key):
            return keys.setdefault(key, len(keys))

        def send(key, src, dst, device):
            k = index(key)
            copy = pltpu.make_async_remote_copy(
                src_ref=src, dst_ref=dst, send_sem=send_sems.at[k], recv_sem=recv_sems.at[k],
                device_id=device, device_id_type=MESH,
            )
            copy.start()
            sent.append(copy)

        def wait(key, dst):
            k = index(key)
            pltpu.make_async_remote_copy(
                src_ref=dst, dst_ref=dst, send_sem=send_sems.at[k], recv_sem=recv_sems.at[k],
                device_id=to_t, device_id_type=MESH,
            ).wait_recv()

        chunks = PARTS - 1 if inside else 1
        first = part if inside else 0
        other_chunks = PARTS - chunks
        other_first = 0 if inside else part
        units = 3 * chunks
        w_load = []
        for u in range(units):
            c, w = u // 3, u % 3
            w_load.append(pltpu.make_async_copy(
                hbm[w].at[:, pl.ds(first + c * part, part)],
                wts.at[u, pl.ds(al(fs * rows, rows), rows)], local_sems.at[2 + u],
            ))
            w_load[u].start()
        ow_load = pltpu.make_async_copy(
            outw_hbm, outw.at[pl.ds(al(fs * rows, rows), rows)], local_sems.at[1])
        ow_load.start()

        def wrow(u, f, off, n):
            return wts.at[u, pl.ds(al(f * rows + off, 128), n)]

        def orow(f, off, n):
            return outw.at[pl.ds(al(f * rows + off, 128), n)]

        def trow(h, t):
            return pl.ds(al(h * hseq + t * (hseq // 2), 64), hseq // 2)

        def tok_z(h):
            send(("tz", h), tok_hbm.at[trow(h, tp)], tok.at[1, trow(h, tp)], to_z)

        def tok_f(h):
            here = tok.at[1, trow(h, tp)]
            wait(("tz", h), here)
            send(("tt", h), here, here, to_t)

        def tok_w(h):
            wait(("tt", h), tok.at[1, trow(h, 1 - tp)])

        def gcols(t, base, c):
            return pl.ds(al(t * cols + base + c * part, 128), part)

        def grow(h):
            return pl.ds(h * hseq, hseq)

        def own_gate(c, finish=True):
            def store(r, x):
                gat[r, gcols(tp, first, c)] = x
            gate(c, first, 0, 0, 2, store)
            here = gat.at[:, gcols(tp, first, c)]
            send(("gt", c, inside), here, here, to_t)

        def partner_gate(c, h):
            def store(r, x):
                mine[c, r, :] = x
            gate(c, first, 1, h, 1, store)
            send(("gz", c, h, inside), mine.at[c, grow(h)], gat.at[grow(h), gcols(tp, first, c)], to_z)

        def take(c, h):
            here = gat.at[grow(h), gcols(tp, other_first, c)]
            wait(("gz", c, h, not inside), here)
            send(("gf", c, h, inside), here, here, to_t)

        def own_other(c):
            wait(("gt", c, inside), gat.at[:, gcols(1 - tp, first, c)])

        def take_other(c, h):
            wait(("gf", c, h, inside), gat.at[grow(h), gcols(1 - tp, other_first, c)])

        f_off, g_off, c_off = m * hrows, (1 - m) * hrows, (1 - m) * 3 * qrows

        if inside:
            pl.semaphore_signal(barrier, inc=1, device_id=to_m, device_id_type=MESH)
            pl.semaphore_wait(barrier, 5)
            hx, hy = m * hrows, (1 - m) * hrows
            woff = m * qrows

            def direct(u):
                c, w = u // 3, u % 3
                at = pl.ds(first + c * part, part)
                send(("dx", u), hbm[w].at[pl.ds(al(hx, 128), hrows), at], wrow(u, fs, hx, hrows), to_x)
                send(("dy", u), hbm[w].at[pl.ds(al(hy, 128), hrows), at], wrow(u, fs, hy, hrows), to_y)

            def relay(u):
                wait(("dx", u), wrow(u, fx, hx, hrows))
                wait(("dy", u), wrow(u, fy, hy, hrows))
                bx, by = wrow(u, fx, hx, hrows), wrow(u, fy, hy, hrows)
                send(("mx", u), bx, bx, to_m)
                send(("rx", u), by, by, to_x)
                send(("ry", u), bx, bx, to_y)
                send(("my", u), by, by, to_m)

            def ready(u):
                w_load[u].wait()
                wait(("rx", u), wrow(u, fd, hy, hrows))
                wait(("ry", u), wrow(u, fd, hx, hrows))
                wait(("mx", u), wrow(u, fx, hrows - hx, hrows))
                wait(("my", u), wrow(u, fy, hrows - hy, hrows))

            tok_z(0)
            tok_z(1)
            for u in range(3):
                direct(u)
            tok_load.wait()
            norm(0, 0, 2)
            relay(0)
            direct(3)
            relay(1)
            direct(4)
            relay(2)
            direct(5)
            ready(0)
            project([0], [0, 1])
            relay(3)
            direct(6)
            ready(1)
            project([1], [0, 1])
            tok_f(0)
            relay(4)
            direct(7)
            tok_w(0)
            norm(1, 0, 1)
            ready(2)
            project([2], [0, 1])
            project([0, 1, 2], [2])
            partner_gate(0, 0)
            own_gate(0)
            relay(5)
            direct(8)
            ready(3)
            project([3], [0, 1, 2])
            relay(6)
            ready(4)
            project([4], [0, 1, 2])
            tok_f(1)
            relay(7)
            tok_w(1)
            norm(1, 1, 1)
            project([0, 1, 2], [3])
            partner_gate(0, 1)
            relay(8)
            for b in range(3):
                off = woff + b * qrows
                src = outw_hbm.at[pl.ds(al(off, 128), qrows)]
                send(("ox", b), src, orow(fs, off, qrows), to_x)
                send(("oy", b), src, orow(fs, off, qrows), to_y)
            ready(5)
            project([5], [0, 1, 2])
            partner_gate(1, 0)
            project([3, 4, 5], [3])
            partner_gate(1, 1)
            own_gate(1)
            block = orow(fd, f_off, hrows)
            wait(("oz", 0), block)
            send(("om",), block, block, to_m)
            ready(6)
            project([6], [0, 1, 2, 3])
            ready(7)
            project([7], [0, 1, 2, 3])
            ready(8)
            project([8], [2])
            partner_gate(2, 0)
            project([8], [3])
            partner_gate(2, 1)
            project([8], [0, 1])
            own_gate(2)
            for h in range(2):
                take(0, h)
            ow_load.wait()
            for c in range(chunks):
                own_other(c)
            for h in range(2):
                take_other(0, h)
            big = hseq
            mix(big, 0, 2, [(al(fs * rows, rows), rows), (al(fd * rows + f_off, 128), hrows)], True, False)
            for b in range(2):
                off = woff + b * qrows
                wait(("ox", b), orow(fx, off, qrows))
                wait(("oy", b), orow(fy, off, qrows))
            mix(big, 0, 2, [(al(f * rows + woff, 128), hrows) for f in (fx, fy)], False, False)
            wait(("oz", 1), orow(fq, c_off, qrows))
            wait(("oz", 2), orow(fp, c_off, qrows))
            wait(("om",), orow(fd, g_off, hrows))
            mix(big, 0, 2, [(al(f * rows + c_off, 128), qrows) for f in (fx, fy)]
                + [(al(fd * rows + g_off, 128), hrows)], False, False)
            off = woff + 2 * qrows
            wait(("ox", 2), orow(fx, off, qrows))
            wait(("oy", 2), orow(fy, off, qrows))
            mix(big, 0, 2, [(al(f * rows + off, 128), qrows) for f in (fx, fy)], False, True)
        else:
            pl.semaphore_wait(barrier, 4)

            def direct(u, which):
                c, w = u // 3, u % 3
                src = hbm[w].at[:, pl.ds(first + c * part, part)]
                send(("d" + which, u), src, wrow(u, fs, 0, rows), to_p if which == "p" else to_q)

            def relay_q(u):
                wait(("dp", u), wrow(u, fp, 0, rows))
                block = wrow(u, fp, f_off, hrows)
                send(("rq", u), block, block, to_q)

            def relay_p(u):
                wait(("dq", u), wrow(u, fq, 0, rows))
                block = wrow(u, fq, g_off, hrows)
                send(("rp", u), block, block, to_p)

            def ready(u):
                w_load[u].wait()
                wait(("rq", u), wrow(u, fd, f_off, hrows))
                wait(("rp", u), wrow(u, fd, g_off, hrows))

            def out_rows(off):
                return outw_hbm.at[pl.ds(al(off, 128), hrows)]

            tok_z(0)
            tok_z(1)
            send(("op", 0), out_rows(f_off), orow(fs, f_off, hrows), to_p)
            for u in range(3):
                direct(u, "q")
                direct(u, "p")
            tok_load.wait()
            norm(0, 0, 2)
            relay_p(0)
            relay_p(1)
            block = orow(fp, f_off, hrows)
            wait(("op", 0), block)
            send(("orq",), block, block, to_q)
            relay_p(2)
            send(("op", 1), out_rows(g_off), orow(fs, g_off, hrows), to_p)
            relay_q(0)
            tok_f(0)
            relay_q(1)
            tok_w(0)
            norm(1, 0, 1)
            relay_q(2)
            send(("oq", 0), out_rows(g_off), orow(fs, g_off, hrows), to_q)
            send(("oq", 1), out_rows(f_off), orow(fs, f_off, hrows), to_q)
            block = orow(fd, f_off, hrows)
            wait(("orq",), block)
            send(("oz", 0), block, block, to_z)
            for u in range(2):
                ready(u)
                project([u], [0, 1, 2])
            tok_f(1)
            ready(2)
            project([2], [2])
            partner_gate(0, 0)
            tok_w(1)
            norm(1, 1, 1)
            project([0, 1, 2], [3])
            partner_gate(0, 1)
            project([2], [0, 1])
            own_gate(0)
            wait(("op", 1), orow(fp, g_off, hrows))
            block = orow(fp, c_off, qrows)
            send(("oz", 2), block, block, to_z)
            block = orow(fq, g_off, hrows)
            wait(("oq", 0), block)
            send(("orp",), block, block, to_p)
            block = orow(fq, c_off, qrows)
            send(("oz", 1), block, block, to_z)
            own_other(0)
            for h in range(2):
                take(0, h)
            wait(("oq", 1), orow(fq, f_off, hrows))
            ow_load.wait()
            for h in range(2):
                take_other(0, h)
            for h in range(2):
                take(1, h)
            wait(("orp",), orow(fd, g_off, hrows))
            mix(hseq, 0, 2, [(0, 2 * part), (cols, 2 * part)], True, False)
            for h in range(2):
                take_other(1, h)
            mix(hseq, 0, 2, [(2 * part, part), (cols + 2 * part, part)], False, False)
            for h in range(2):
                take(2, h)
                take_other(2, h)
                mix(hseq, h, 1, [(3 * part, part), (cols + 3 * part, part)], False, True)

        for copy in sent:
            copy.wait_send()

    @pl.when(inner_chip == 1)
    def _():
        program(True)

    @pl.when(inner_chip == 0)
    def _():
        program(False)

    assert len(keys) <= COPIES


def paired(tokens, norm_gain, outer_weight, inner_weight, value_weight, conv_taps, out_weight):
    _, seq, width = tokens.shape
    rows, cols = outer_weight.shape
    part = cols // PARTS
    anyspace = pl.BlockSpec(memory_space=pltpu.HBM)
    vmem = pl.BlockSpec(memory_space=pltpu.VMEM)
    out = pl.pallas_call(
        kernel,
        out_shape=pltpu.VMEM((seq, cols), BF16),
        in_specs=[anyspace, vmem, anyspace, anyspace, anyspace, vmem, anyspace],
        out_specs=vmem,
        scratch_shapes=[
            pltpu.VMEM((2, seq, width), BF16),
            pltpu.VMEM((2 * seq, width), BF16),
            pltpu.VMEM((3 * (PARTS - 1), width, part), BF16),
            pltpu.VMEM((width, cols), BF16),
            pltpu.VMEM((3, PARTS - 1, 2, seq + PAD, part), BF16),
            pltpu.VMEM((seq, width), BF16),
            pltpu.VMEM((PARTS - 1, seq, part), BF16),
            pltpu.VMEM((seq, cols), F32),
            pltpu.SemaphoreType.DMA((COPIES,)),
            pltpu.SemaphoreType.DMA((COPIES,)),
            pltpu.SemaphoreType.DMA((2 + 3 * (PARTS - 1),)),
        ],
        compiler_params=pltpu.CompilerParams(
            collective_id=0, has_side_effects=True, vmem_limit_bytes=58 * 1024 * 1024
        ),
        name="mixer",
    )(
        tokens.reshape(seq, width), norm_gain.reshape(1, width), outer_weight, inner_weight,
        value_weight, conv_taps, out_weight,
    )
    return out.reshape(1, seq, cols)


def solution(mesh):
    shape = dict(mesh.shape)

    def local(tokens, *rest):
        rows, cols = rest[1].shape
        fits = (
            shape["fs"] == 4 and shape["tp"] == 2 and shape["rep"] == 4
            and tokens.shape[0] == 1 and tokens.shape[1] % 256 == 0
            and rows % 512 == 0 and cols == 2 * rows and rest[4].shape[0] <= 9
        )
        return (paired if fits else plain)(tokens, *rest)

    in_specs = (
        P(("rep", "fs"), None, None),
        P(),
        P("fs", "tp"),
        P("fs", "tp"),
        P("fs", "tp"),
        P(),
        P("fs", "tp"),
    )
    out_specs = P(("rep", "fs"), None, "tp")
    return jax.shard_map(local, mesh=mesh, in_specs=in_specs, out_specs=out_specs, check_vma=False)
```

time: 85.2 us -> 77.7 us (0.912); the launches traced: 84.1 us -> 77.5 us
  Pallas kernels: 82.9 us -> 76.3 us
    pallas_call x1, Pallas kernels: 82.9 us -> 76.3 us  [paired(): pl.pallas_call(kernel, out_shape=pltpu.VMEM((seq, cols), BF16), in_specs=...]
where the time goes in v1:
time: 77.7 us; the launch traced here: 77.5 us
  Pallas kernels  76.3 us (98%)
  local copies, waits for them, and re-layouts  1.15 us (1%)
    pallas_call x1, Pallas kernels, paired(): pl.pallas_call(kernel, out_shape=pltpu.VMEM((seq, cols), BF16), in_specs=...  76.3 us

profile of v1, /device:TPU:9, one launch (start us, length us, event | category | flops | bytes accessed | tf_op | source)
XLA Modules:
  0.0 77.5 jit_solution(3355757378681028320)
XLA Ops:
  0.0 76.3 %mixer.1 = bf16[768,1024]{1,0:T(8,128)(2,1)S(1)} custom-call(bf16[768,2048]{1,0:T(8,128)(2,1)} %bitcast.4, f32[1,2048]{1,0:T(1,128)} %bitcast.5, bf16[512,1024]{1,0:T(8,128)(2,1)} %outer_hbm.1, bf16[512,1024]{1,0:T(8,128)(2,1)} %inner_hbm.1, bf16[512,1024]{1,0:T(8,128)(2,1)} %value_hbm.1, f32[3,2048]{1,0:T(4,128)} %taps_ref.1, bf16[512,1024]{1,0:T(8,128)(2,1)} %outw_hbm.1), custom_call_target="tpu_custom_call" | custom-call | tf_op jit(solution)/shard_map/mixer/pallas_call | solution.py:460
  76.3 1.1 %copy.9 = bf16[1,768,1024]{2,1,0:T(8,128)(2,1)} copy(bf16[1,768,1024]{2,1,0:T(8,128)(2,1)S(1)} %bitcast.3) | data formatting | bytes 3145728

commit v2 on v1

--- a/solution.py
+++ b/solution.py
@@ -39,12 +39,13 @@
 
 PARTS = 4
 PAD = 16
-COPIES = 112
+CROSS = 9
+COPIES = CROSS + 24
 
 
 def kernel(
-    tok_hbm, gain_ref, outer_hbm, inner_hbm, value_hbm, taps_ref, outw_hbm, out_ref,
-    tok, nm, wts, outw, proj, gat, mine, osum, send_sems, recv_sems, local_sems,
+    tok_hbm, gain_hbm, outer_hbm, inner_hbm, value_hbm, taps_hbm, outw_hbm, out_ref,
+    gain_ref, taps_ref, tok, nm, wts, outw, proj, gat, mine, osum, send_sems, recv_sems, local_sems,
 ):
     rep, fs, tp = lax.axis_index("rep"), lax.axis_index("fs"), lax.axis_index("tp")
     seq, width = tok_hbm.shape
@@ -64,7 +65,7 @@
     to_x, to_y, to_p, to_q = (rep, fx, tp), (rep, fy, tp), (rep, fp, tp), (rep, fq, tp)
     to_z, to_t = (rep + 1 - 2 * lax.rem(rep, 2), fs, tp), (rep, fs, 1 - tp)
     to_m = (3 - rep, fs, tp)
-    keys = {}
+    cross = {}
 
     barrier = pltpu.get_barrier_semaphore()
     for peer in (to_x, to_y, to_z, to_t):
@@ -72,6 +73,10 @@
 
     hbm = (inner_hbm, value_hbm, outer_hbm)
     tok_load = pltpu.make_async_copy(tok_hbm, tok.at[0], local_sems.at[0])
+    gain_load = pltpu.make_async_copy(gain_hbm, gain_ref, local_sems.at[1])
+    taps_load = pltpu.make_async_copy(taps_hbm, taps_ref, local_sems.at[2])
+    gain_load.start()
+    taps_load.start()
     tok_load.start()
 
     def al(x, n):
@@ -137,42 +142,48 @@
                 osum[r, :] = total
 
     def program(inside):
-        sent = []
+        local = {}
 
         def index(key):
-            return keys.setdefault(key, len(keys))
-
-        def send(key, src, dst, device):
+            if key[0] in ("tz", "gz", "oz"):
+                return cross.setdefault(key, len(cross))
+            return CROSS + local.setdefault(key, len(local))
+
+        def send(key, src, dst, device, group):
             k = index(key)
-            copy = pltpu.make_async_remote_copy(
-                src_ref=src, dst_ref=dst, send_sem=send_sems.at[k], recv_sem=recv_sems.at[k],
+            pltpu.make_async_remote_copy(
+                src_ref=src, dst_ref=dst, send_sem=send_sems.at[group], recv_sem=recv_sems.at[k],
                 device_id=device, device_id_type=MESH,
-            )
-            copy.start()
-            sent.append(copy)
+            ).start()
 
         def wait(key, dst):
             k = index(key)
             pltpu.make_async_remote_copy(
-                src_ref=dst, dst_ref=dst, send_sem=send_sems.at[k], recv_sem=recv_sems.at[k],
+                src_ref=dst, dst_ref=dst, send_sem=send_sems.at[0], recv_sem=recv_sems.at[k],
                 device_id=to_t, device_id_type=MESH,
             ).wait_recv()
+
+        def wait_sent(group, src):
+            pltpu.make_async_remote_copy(
+                src_ref=src, dst_ref=src, send_sem=send_sems.at[group], recv_sem=recv_sems.at[0],
+                device_id=to_t, device_id_type=MESH,
+            ).wait_send()
 
         chunks = PARTS - 1 if inside else 1
         first = part if inside else 0
         other_chunks = PARTS - chunks
         other_first = 0 if inside else part
         units = 3 * chunks
-        w_load = []
         for u in range(units):
             c, w = u // 3, u % 3
-            w_load.append(pltpu.make_async_copy(
+            pltpu.make_async_copy(
                 hbm[w].at[:, pl.ds(first + c * part, part)],
-                wts.at[u, pl.ds(al(fs * rows, rows), rows)], local_sems.at[2 + u],
-            ))
-            w_load[u].start()
+                wts.at[u, pl.ds(al(fs * rows, rows), rows)], local_sems.at[3],
+            ).start()
+        w_load = pltpu.make_async_copy(
+            wts.at[0:units, 0:rows], wts.at[0:units, 0:rows], local_sems.at[3])
         ow_load = pltpu.make_async_copy(
-            outw_hbm, outw.at[pl.ds(al(fs * rows, rows), rows)], local_sems.at[1])
+            outw_hbm, outw.at[pl.ds(al(fs * rows, rows), rows)], local_sems.at[4])
         ow_load.start()
 
         def wrow(u, f, off, n):
@@ -185,12 +196,12 @@
             return pl.ds(al(h * hseq + t * (hseq // 2), 64), hseq // 2)
 
         def tok_z(h):
-            send(("tz", h), tok_hbm.at[trow(h, tp)], tok.at[1, trow(h, tp)], to_z)
+            send(("tz", h), tok_hbm.at[trow(h, tp)], tok.at[1, trow(h, tp)], to_z, 1)
 
         def tok_f(h):
             here = tok.at[1, trow(h, tp)]
             wait(("tz", h), here)
-            send(("tt", h), here, here, to_t)
+            send(("tt", h), here, here, to_t, 1)
 
         def tok_w(h):
             wait(("tt", h), tok.at[1, trow(h, 1 - tp)])
@@ -199,31 +210,31 @@
             return pl.ds(al(t * cols + base + c * part, 128), part)
 
         def grow(h):
-            return pl.ds(h * hseq, hseq)
-
-        def own_gate(c, finish=True):
+            return pl.ds(0, seq) if h is None else pl.ds(h * hseq, hseq)
+
+        def z_key(c, h, from_inside):
+            return ("gz", c, h if from_inside and c == PARTS - 2 else None, from_inside)
+
+        def own_gate(c, key):
             def store(r, x):
                 gat[r, gcols(tp, first, c)] = x
             gate(c, first, 0, 0, 2, store)
             here = gat.at[:, gcols(tp, first, c)]
-            send(("gt", c, inside), here, here, to_t)
+            send(key, here, here, to_t, 3)
 
         def partner_gate(c, h):
             def store(r, x):
                 mine[c, r, :] = x
-            gate(c, first, 1, h, 1, store)
-            send(("gz", c, h, inside), mine.at[c, grow(h)], gat.at[grow(h), gcols(tp, first, c)], to_z)
-
-        def take(c, h):
+            gate(c, first, 1, h or 0, 2 if h is None else 1, store)
+            send(z_key(c, h, inside), mine.at[c, grow(h)], gat.at[grow(h), gcols(tp, first, c)], to_z, 3)
+
+        def take(c, h, key):
             here = gat.at[grow(h), gcols(tp, other_first, c)]
-            wait(("gz", c, h, not inside), here)
-            send(("gf", c, h, inside), here, here, to_t)
-
-        def own_other(c):
-            wait(("gt", c, inside), gat.at[:, gcols(1 - tp, first, c)])
-
-        def take_other(c, h):
-            wait(("gf", c, h, inside), gat.at[grow(h), gcols(1 - tp, other_first, c)])
+            wait(z_key(c, h, not inside), here)
+            send(key, here, here, to_t, 3)
+
+        def take_other(key, h, parts):
+            wait(key, gat.at[grow(h), pl.ds(0, parts * part)])
 
         f_off, g_off, c_off = m * hrows, (1 - m) * hrows, (1 - m) * 3 * qrows
 
@@ -236,30 +247,28 @@
             def direct(u):
                 c, w = u // 3, u % 3
                 at = pl.ds(first + c * part, part)
-                send(("dx", u), hbm[w].at[pl.ds(al(hx, 128), hrows), at], wrow(u, fs, hx, hrows), to_x)
-                send(("dy", u), hbm[w].at[pl.ds(al(hy, 128), hrows), at], wrow(u, fs, hy, hrows), to_y)
+                send(("d", u), hbm[w].at[pl.ds(al(hx, 128), hrows), at], wrow(u, fs, hx, hrows), to_x, 0)
+                send(("d", u), hbm[w].at[pl.ds(al(hy, 128), hrows), at], wrow(u, fs, hy, hrows), to_y, 0)
 
             def relay(u):
-                wait(("dx", u), wrow(u, fx, hx, hrows))
-                wait(("dy", u), wrow(u, fy, hy, hrows))
+                wait(("d", u), wts.at[u, 0 : 2 * hrows])
                 bx, by = wrow(u, fx, hx, hrows), wrow(u, fy, hy, hrows)
-                send(("mx", u), bx, bx, to_m)
-                send(("rx", u), by, by, to_x)
-                send(("ry", u), bx, bx, to_y)
-                send(("my", u), by, by, to_m)
+                send(("r", u), bx, bx, to_m, 0)
+                send(("r", u), by, by, to_x, 0)
+                send(("r", u), bx, bx, to_y, 0)
+                send(("r", u), by, by, to_m, 0)
 
             def ready(u):
-                w_load[u].wait()
-                wait(("rx", u), wrow(u, fd, hy, hrows))
-                wait(("ry", u), wrow(u, fd, hx, hrows))
-                wait(("mx", u), wrow(u, fx, hrows - hx, hrows))
-                wait(("my", u), wrow(u, fy, hrows - hy, hrows))
+                if u == 0:
+                    w_load.wait()
+                wait(("r", u), wts.at[u, 0 : 4 * hrows])
 
             tok_z(0)
             tok_z(1)
             for u in range(3):
                 direct(u)
             tok_load.wait()
+            gain_load.wait()
             norm(0, 0, 2)
             relay(0)
             direct(3)
@@ -281,8 +290,9 @@
             ready(2)
             project([2], [0, 1])
             project([0, 1, 2], [2])
+            taps_load.wait()
             partner_gate(0, 0)
-            own_gate(0)
+            own_gate(0, ("ga",))
             relay(5)
             direct(8)
             ready(3)
@@ -300,17 +310,17 @@
             for b in range(3):
                 off = woff + b * qrows
                 src = outw_hbm.at[pl.ds(al(off, 128), qrows)]
-                send(("ox", b), src, orow(fs, off, qrows), to_x)
-                send(("oy", b), src, orow(fs, off, qrows), to_y)
+                send(("o", b), src, orow(fs, off, qrows), to_x, 2)
+                send(("o", b), src, orow(fs, off, qrows), to_y, 2)
             ready(5)
             project([5], [0, 1, 2])
             partner_gate(1, 0)
             project([3, 4, 5], [3])
             partner_gate(1, 1)
-            own_gate(1)
+            own_gate(1, ("ga",))
             block = orow(fd, f_off, hrows)
             wait(("oz", 0), block)
-            send(("om",), block, block, to_m)
+            send(("oz", 1), block, block, to_m, 2)
             ready(6)
             project([6], [0, 1, 2, 3])
             ready(7)
@@ -321,124 +331,116 @@
             project([8], [3])
             partner_gate(2, 1)
             project([8], [0, 1])
-            own_gate(2)
-            for h in range(2):
-                take(0, h)
+            own_gate(2, ("ga",))
+            take(0, None, ("ga",))
             ow_load.wait()
-            for c in range(chunks):
-                own_other(c)
-            for h in range(2):
-                take_other(0, h)
+            take_other(("ga",), None, PARTS)
             big = hseq
             mix(big, 0, 2, [(al(fs * rows, rows), rows), (al(fd * rows + f_off, 128), hrows)], True, False)
             for b in range(2):
-                off = woff + b * qrows
-                wait(("ox", b), orow(fx, off, qrows))
-                wait(("oy", b), orow(fy, off, qrows))
+                wait(("o", b), outw.at[0 : 2 * qrows])
             mix(big, 0, 2, [(al(f * rows + woff, 128), hrows) for f in (fx, fy)], False, False)
-            wait(("oz", 1), orow(fq, c_off, qrows))
-            wait(("oz", 2), orow(fp, c_off, qrows))
-            wait(("om",), orow(fd, g_off, hrows))
+            wait(("oz", 1), outw.at[0 : 4 * qrows])
             mix(big, 0, 2, [(al(f * rows + c_off, 128), qrows) for f in (fx, fy)]
                 + [(al(fd * rows + g_off, 128), hrows)], False, False)
             off = woff + 2 * qrows
-            wait(("ox", 2), orow(fx, off, qrows))
-            wait(("oy", 2), orow(fy, off, qrows))
+            wait(("o", 2), outw.at[0 : 2 * qrows])
             mix(big, 0, 2, [(al(f * rows + off, 128), qrows) for f in (fx, fy)], False, True)
+            wait_sent(0, wts.at[:, 0 : 6 * hrows])
+            wait_sent(1, tok.at[0])
+            wait_sent(2, outw.at[0 : 8 * qrows])
+            wait_sent(3, gat.at[:, 0 : 7 * part])
         else:
             pl.semaphore_wait(barrier, 4)
 
             def direct(u, which):
                 c, w = u // 3, u % 3
                 src = hbm[w].at[:, pl.ds(first + c * part, part)]
-                send(("d" + which, u), src, wrow(u, fs, 0, rows), to_p if which == "p" else to_q)
+                send(("d" + which, u), src, wrow(u, fs, 0, rows), to_p if which == "p" else to_q, 0)
 
             def relay_q(u):
                 wait(("dp", u), wrow(u, fp, 0, rows))
                 block = wrow(u, fp, f_off, hrows)
-                send(("rq", u), block, block, to_q)
+                send(("r", u), block, block, to_q, 0)
 
             def relay_p(u):
                 wait(("dq", u), wrow(u, fq, 0, rows))
                 block = wrow(u, fq, g_off, hrows)
-                send(("rp", u), block, block, to_p)
+                send(("r", u), block, block, to_p, 0)
 
             def ready(u):
-                w_load[u].wait()
-                wait(("rq", u), wrow(u, fd, f_off, hrows))
-                wait(("rp", u), wrow(u, fd, g_off, hrows))
+                if u == 0:
+                    w_load.wait()
+                wait(("r", u), wts.at[u, 0 : 2 * hrows])
 
             def out_rows(off):
                 return outw_hbm.at[pl.ds(al(off, 128), hrows)]
 
             tok_z(0)
             tok_z(1)
-            send(("op", 0), out_rows(f_off), orow(fs, f_off, hrows), to_p)
+            send(("op", 0), out_rows(f_off), orow(fs, f_off, hrows), to_p, 2)
             for u in range(3):
                 direct(u, "q")
                 direct(u, "p")
             tok_load.wait()
+            gain_load.wait()
             norm(0, 0, 2)
             relay_p(0)
             relay_p(1)
             block = orow(fp, f_off, hrows)
             wait(("op", 0), block)
-            send(("orq",), block, block, to_q)
+            send(("orq",), block, block, to_q, 2)
             relay_p(2)
-            send(("op", 1), out_rows(g_off), orow(fs, g_off, hrows), to_p)
+            send(("op", 1), out_rows(g_off), orow(fs, g_off, hrows), to_p, 2)
             relay_q(0)
             tok_f(0)
             relay_q(1)
             tok_w(0)
             norm(1, 0, 1)
             relay_q(2)
-            send(("oq", 0), out_rows(g_off), orow(fs, g_off, hrows), to_q)
-            send(("oq", 1), out_rows(f_off), orow(fs, f_off, hrows), to_q)
+            send(("oq", 0), out_rows(g_off), orow(fs, g_off, hrows), to_q, 2)
+            send(("oq", 1), out_rows(f_off), orow(fs, f_off, hrows), to_q, 2)
             block = orow(fd, f_off, hrows)
             wait(("orq",), block)
-            send(("oz", 0), block, block, to_z)
+            send(("oz", 0), block, block, to_z, 2)
             for u in range(2):
                 ready(u)
                 project([u], [0, 1, 2])
             tok_f(1)
             ready(2)
             project([2], [2])
-            partner_gate(0, 0)
+            taps_load.wait()
             tok_w(1)
             norm(1, 1, 1)
             project([0, 1, 2], [3])
-            partner_gate(0, 1)
+            partner_gate(0, None)
             project([2], [0, 1])
-            own_gate(0)
+            own_gate(0, ("ga",))
             wait(("op", 1), orow(fp, g_off, hrows))
             block = orow(fp, c_off, qrows)
-            send(("oz", 2), block, block, to_z)
+            send(("oz", 1), block, block, to_z, 2)
             block = orow(fq, g_off, hrows)
             wait(("oq", 0), block)
-            send(("orp",), block, block, to_p)
+            send(("orp",), block, block, to_p, 2)
             block = orow(fq, c_off, qrows)
-            send(("oz", 1), block, block, to_z)
-            own_other(0)
-            for h in range(2):
-                take(0, h)
+            send(("oz", 1), block, block, to_z, 2)
+            take(0, None, ("ga",))
             wait(("oq", 1), orow(fq, f_off, hrows))
             ow_load.wait()
-            for h in range(2):
-                take_other(0, h)
-            for h in range(2):
-                take(1, h)
+            take_other(("ga",), None, 2)
+            take(1, None, ("gb",))
             wait(("orp",), orow(fd, g_off, hrows))
             mix(hseq, 0, 2, [(0, 2 * part), (cols, 2 * part)], True, False)
-            for h in range(2):
-                take_other(1, h)
+            take_other(("gb",), None, 1)
             mix(hseq, 0, 2, [(2 * part, part), (cols + 2 * part, part)], False, False)
             for h in range(2):
-                take(2, h)
-                take_other(2, h)
+                take(2, h, ("gc", h))
+                take_other(("gc", h), h, 1)
                 mix(hseq, h, 1, [(3 * part, part), (cols + 3 * part, part)], False, True)
-
-        for copy in sent:
-            copy.wait_send()
+            wait_sent(0, wts.at[0:units, 0 : 6 * hrows])
+            wait_sent(1, tok.at[0])
+            wait_sent(2, outw)
+            wait_sent(3, gat.at[:, 0 : 5 * part])
 
     @pl.when(inner_chip == 1)
     def _():
@@ -448,7 +450,7 @@
     def _():
         program(False)
 
-    assert len(keys) <= COPIES
+    assert len(cross) <= CROSS
 
 
 def paired(tokens, norm_gain, outer_weight, inner_weight, value_weight, conv_taps, out_weight):
@@ -460,9 +462,11 @@
     out = pl.pallas_call(
         kernel,
         out_shape=pltpu.VMEM((seq, cols), BF16),
-        in_specs=[anyspace, vmem, anyspace, anyspace, anyspace, vmem, anyspace],
+        in_specs=[anyspace] * 7,
         out_specs=vmem,
         scratch_shapes=[
+            pltpu.VMEM((1, width), F32),
+            pltpu.VMEM(conv_taps.shape, F32),
             pltpu.VMEM((2, seq, width), BF16),
             pltpu.VMEM((2 * seq, width), BF16),
             pltpu.VMEM((3 * (PARTS - 1), width, part), BF16),
@@ -471,9 +475,9 @@
             pltpu.VMEM((seq, width), BF16),
             pltpu.VMEM((PARTS - 1, seq, part), BF16),
             pltpu.VMEM((seq, cols), F32),
+            pltpu.SemaphoreType.DMA((4,)),
             pltpu.SemaphoreType.DMA((COPIES,)),
-            pltpu.SemaphoreType.DMA((COPIES,)),
-            pltpu.SemaphoreType.DMA((2 + 3 * (PARTS - 1),)),
+            pltpu.SemaphoreType.DMA((5,)),
         ],
         compiler_params=pltpu.CompilerParams(
             collective_id=0, has_side_effects=True, vmem_limit_bytes=58 * 1024 * 1024

time: 77.7 us -> 75 us (0.965)
  Pallas kernels: 76.3 us -> 73.7 us
    pallas_call x1, Pallas kernels: 76.3 us -> 73.7 us  [paired(): pl.pallas_call(kernel, out_shape=pltpu.VMEM((seq, cols), BF16), in_specs=...]
where the time goes in v2:
time: 75 us; the launch traced here: 74.9 us
  Pallas kernels  73.7 us (98%)
  local copies, waits for them, and re-layouts  1.15 us (2%)
    pallas_call x1, Pallas kernels, paired(): pl.pallas_call(kernel, out_shape=pltpu.VMEM((seq, cols), BF16), in_specs=...  73.7 us

profile of v2, /device:TPU:9, one launch (start us, length us, event | category | flops | bytes accessed | tf_op | source)
XLA Modules:
  0.0 74.9 jit_solution(18097118073264674334)
XLA Ops:
  0.0 73.7 %mixer.1 = bf16[768,1024]{1,0:T(8,128)(2,1)S(1)} custom-call(bf16[768,2048]{1,0:T(8,128)(2,1)} %bitcast.4, f32[1,2048]{1,0:T(1,128)} %bitcast.5, bf16[512,1024]{1,0:T(8,128)(2,1)} %outer_hbm.1, bf16[512,1024]{1,0:T(8,128)(2,1)} %inner_hbm.1, bf16[512,1024]{1,0:T(8,128)(2,1)} %value_hbm.1, f32[3,2048]{1,0:T(4,128)} %taps_hbm.1, bf16[512,1024]{1,0:T(8,128)(2,1)} %outw_hbm.1), custom_call_target="tpu_custom_call" | custom-call | tf_op jit(solution)/shard_map/mixer/pallas_call | solution.py:462
  73.7 1.1 %copy.9 = bf16[1,768,1024]{2,1,0:T(8,128)(2,1)} copy(bf16[1,768,1024]{2,1,0:T(8,128)(2,1)S(1)} %bitcast.3) | data formatting | bytes 3145728

commit v3 on v2

--- a/solution.py
+++ b/solution.py
@@ -40,7 +40,7 @@
 PARTS = 4
 PAD = 16
 CROSS = 9
-COPIES = CROSS + 24
+COPIES = CROSS + 25
 
 
 def kernel(
@@ -53,7 +53,8 @@
     part = cols // PARTS
     hseq = seq // 2
     hrows = rows // 2
-    qrows = rows // 4
+    crows = rows * 9 // 32
+    orest = hrows - crows
     count = taps_ref.shape[0]
     m = rep // 2
     inner_chip = lax.rem(rep, 2) + m - 2 * lax.rem(rep, 2) * m
@@ -126,20 +127,21 @@
                 conv = conv + taps_ref[k : k + 1, tcols] * window[lo : lo + tile, :]
             store(pl.ds(r, tile), (outer * conv).astype(BF16))
 
-    def mix(tile_rows, b0, nb, terms, first, last):
-        @pl.loop(b0, b0 + nb)
-        def _(b):
-            r = pl.ds(al(b * tile_rows, tile_rows), tile_rows)
+    def mix(h, terms, first, last):
+        r = slice(0, seq) if h is None else slice(h * hseq, (h + 1) * hseq)
+
+        for b in range(cols // part):
+            at = slice(b * part, (b + 1) * part)
             total = None
             for k, n in terms:
-                d = jnp.dot(gat[r, pl.ds(k, n)], outw[pl.ds(k, n), :], preferred_element_type=F32)
+                d = jnp.dot(gat[r, pl.ds(k, n)], outw[pl.ds(k, n), at], preferred_element_type=F32)
                 total = d if total is None else total + d
             if not first:
-                total = total + osum[r, :]
+                total = total + osum[r, at]
             if last:
-                out_ref[r, :] = total.astype(BF16)
+                out_ref[r, at] = total.astype(BF16)
             else:
-                osum[r, :] = total
+                osum[r, at] = total
 
     def program(inside):
         local = {}
@@ -190,7 +192,7 @@
             return wts.at[u, pl.ds(al(f * rows + off, 128), n)]
 
         def orow(f, off, n):
-            return outw.at[pl.ds(al(f * rows + off, 128), n)]
+            return outw.at[pl.ds(al(f * rows + off, 16), n)]
 
         def trow(h, t):
             return pl.ds(al(h * hseq + t * (hseq // 2), 64), hseq // 2)
@@ -236,13 +238,13 @@
         def take_other(key, h, parts):
             wait(key, gat.at[grow(h), pl.ds(0, parts * part)])
 
-        f_off, g_off, c_off = m * hrows, (1 - m) * hrows, (1 - m) * 3 * qrows
+        f_off, g_off = m * hrows, (1 - m) * hrows
+        c_off, o_off = g_off + (1 - m) * orest, g_off + m * crows
 
         if inside:
             pl.semaphore_signal(barrier, inc=1, device_id=to_m, device_id_type=MESH)
             pl.semaphore_wait(barrier, 5)
             hx, hy = m * hrows, (1 - m) * hrows
-            woff = m * qrows
 
             def direct(u):
                 c, w = u // 3, u % 3
@@ -307,20 +309,23 @@
             project([0, 1, 2], [3])
             partner_gate(0, 1)
             relay(8)
-            for b in range(3):
-                off = woff + b * qrows
-                src = outw_hbm.at[pl.ds(al(off, 128), qrows)]
-                send(("o", b), src, orow(fs, off, qrows), to_x, 2)
-                send(("o", b), src, orow(fs, off, qrows), to_y, 2)
+            for b, (off, n) in enumerate(((f_off, hrows), (o_off, orest))):
+                src = outw_hbm.at[pl.ds(al(off, 16), n)]
+                send(("o", b), src, orow(fs, off, n), to_x, 2)
+                send(("o", b), src, orow(fs, off, n), to_y, 2)
             ready(5)
             project([5], [0, 1, 2])
             partner_gate(1, 0)
             project([3, 4, 5], [3])
             partner_gate(1, 1)
             own_gate(1, ("ga",))
-            block = orow(fd, f_off, hrows)
-            wait(("oz", 0), block)
-            send(("oz", 1), block, block, to_m, 2)
+            wait(("oz", 0), orow(fd, f_off, hrows))
+
+            def swap():
+                block = orow(fd, f_off, hrows)
+                send(("om",), block, block, to_m, 2)
+
+            pl.when(tp == 0)(swap)
             ready(6)
             project([6], [0, 1, 2, 3])
             ready(7)
@@ -330,25 +335,26 @@
             partner_gate(2, 0)
             project([8], [3])
             partner_gate(2, 1)
+            pl.when(tp == 1)(swap)
             project([8], [0, 1])
             own_gate(2, ("ga",))
             take(0, None, ("ga",))
             ow_load.wait()
             take_other(("ga",), None, PARTS)
-            big = hseq
-            mix(big, 0, 2, [(al(fs * rows, rows), rows), (al(fd * rows + f_off, 128), hrows)], True, False)
-            for b in range(2):
-                wait(("o", b), outw.at[0 : 2 * qrows])
-            mix(big, 0, 2, [(al(f * rows + woff, 128), hrows) for f in (fx, fy)], False, False)
-            wait(("oz", 1), outw.at[0 : 4 * qrows])
-            mix(big, 0, 2, [(al(f * rows + c_off, 128), qrows) for f in (fx, fy)]
-                + [(al(fd * rows + g_off, 128), hrows)], False, False)
-            off = woff + 2 * qrows
-            wait(("o", 2), outw.at[0 : 2 * qrows])
-            mix(big, 0, 2, [(al(f * rows + off, 128), qrows) for f in (fx, fy)], False, True)
+            def krow(f, off):
+                return al(f * rows + off, 128), hrows
+
+            mix(None, [(al(fs * rows, rows), rows), krow(fd, f_off)], True, False)
+            wait(("o", 0), outw.at[0 : 2 * hrows])
+            mix(None, [krow(fx, f_off), krow(fy, f_off)], False, False)
+            wait(("om",), orow(fd, g_off, hrows))
+            mix(None, [krow(fd, g_off)], False, False)
+            wait(("oz", 1), outw.at[0 : 2 * crows])
+            wait(("o", 1), outw.at[0 : 2 * orest])
+            mix(None, [krow(fx, g_off), krow(fy, g_off)], False, True)
             wait_sent(0, wts.at[:, 0 : 6 * hrows])
             wait_sent(1, tok.at[0])
-            wait_sent(2, outw.at[0 : 8 * qrows])
+            wait_sent(2, outw.at[0 : 3 * hrows + 2 * orest])
             wait_sent(3, gat.at[:, 0 : 7 * part])
         else:
             pl.semaphore_wait(barrier, 4)
@@ -374,7 +380,7 @@
                 wait(("r", u), wts.at[u, 0 : 2 * hrows])
 
             def out_rows(off):
-                return outw_hbm.at[pl.ds(al(off, 128), hrows)]
+                return outw_hbm.at[pl.ds(al(off, 16), hrows)]
 
             tok_z(0)
             tok_z(1)
@@ -417,30 +423,32 @@
             project([2], [0, 1])
             own_gate(0, ("ga",))
             wait(("op", 1), orow(fp, g_off, hrows))
-            block = orow(fp, c_off, qrows)
-            send(("oz", 1), block, block, to_z, 2)
+            block = orow(fp, c_off, crows)
+            send(("oz", 1), block, block, to_z, 4)
             block = orow(fq, g_off, hrows)
             wait(("oq", 0), block)
             send(("orp",), block, block, to_p, 2)
-            block = orow(fq, c_off, qrows)
-            send(("oz", 1), block, block, to_z, 2)
+            block = orow(fq, c_off, crows)
+            send(("oz", 1), block, block, to_z, 4)
             take(0, None, ("ga",))
             wait(("oq", 1), orow(fq, f_off, hrows))
             ow_load.wait()
             take_other(("ga",), None, 2)
             take(1, None, ("gb",))
             wait(("orp",), orow(fd, g_off, hrows))
-            mix(hseq, 0, 2, [(0, 2 * part), (cols, 2 * part)], True, False)
+            mix(None, [(0, 2 * part), (cols, 2 * part)], True, False)
             take_other(("gb",), None, 1)
-            mix(hseq, 0, 2, [(2 * part, part), (cols + 2 * part, part)], False, False)
+            mix(None, [(2 * part, part), (cols + 2 * part, part)], False, False)
             for h in range(2):
                 take(2, h, ("gc", h))
+            for h in range(2):
                 take_other(("gc", h), h, 1)
-                mix(hseq, h, 1, [(3 * part, part), (cols + 3 * part, part)], False, True)
+                mix(h, [(3 * part, part), (cols + 3 * part, part)], False, True)
             wait_sent(0, wts.at[0:units, 0 : 6 * hrows])
             wait_sent(1, tok.at[0])
-            wait_sent(2, outw)
+            wait_sent(2, outw.at[0 : 7 * hrows])
             wait_sent(3, gat.at[:, 0 : 5 * part])
+            wait_sent(4, outw.at[0 : 2 * crows])
 
     @pl.when(inner_chip == 1)
     def _():
@@ -475,7 +483,7 @@
             pltpu.VMEM((seq, width), BF16),
             pltpu.VMEM((PARTS - 1, seq, part), BF16),
             pltpu.VMEM((seq, cols), F32),
-            pltpu.SemaphoreType.DMA((4,)),
+            pltpu.SemaphoreType.DMA((5,)),
             pltpu.SemaphoreType.DMA((COPIES,)),
             pltpu.SemaphoreType.DMA((5,)),
         ],

time: 75 us -> 73.5 us (0.980)
  Pallas kernels: 73.7 us -> 72.2 us
    pallas_call x1, Pallas kernels: 73.7 us -> 72.2 us  [paired(): pl.pallas_call(kernel, out_shape=pltpu.VMEM((seq, cols), BF16), in_specs=...]
where the time goes in v3:
time: 73.5 us; the launch traced here: 73.3 us
  Pallas kernels  72.2 us (98%)
  local copies, waits for them, and re-layouts  1.15 us (2%)
    pallas_call x1, Pallas kernels, paired(): pl.pallas_call(kernel, out_shape=pltpu.VMEM((seq, cols), BF16), in_specs=...  72.2 us

profile of v3, /device:TPU:9, one launch (start us, length us, event | category | flops | bytes accessed | tf_op | source)
XLA Modules:
  0.0 73.3 jit_solution(18227731360390216630)
XLA Ops:
  0.0 72.2 %mixer.1 = bf16[768,1024]{1,0:T(8,128)(2,1)S(1)} custom-call(bf16[768,2048]{1,0:T(8,128)(2,1)} %bitcast.4, f32[1,2048]{1,0:T(1,128)} %bitcast.5, bf16[512,1024]{1,0:T(8,128)(2,1)} %outer_hbm.1, bf16[512,1024]{1,0:T(8,128)(2,1)} %inner_hbm.1, bf16[512,1024]{1,0:T(8,128)(2,1)} %value_hbm.1, f32[3,2048]{1,0:T(4,128)} %taps_hbm.1, bf16[512,1024]{1,0:T(8,128)(2,1)} %outw_hbm.1), custom_call_target="tpu_custom_call" | custom-call | tf_op jit(solution)/shard_map/mixer/pallas_call | solution.py:470
  72.2 1.1 %copy.9 = bf16[1,768,1024]{2,1,0:T(8,128)(2,1)} copy(bf16[1,768,1024]{2,1,0:T(8,128)(2,1)S(1)} %bitcast.3) | data formatting | bytes 3145728

commit v4 on v3

--- a/solution.py
+++ b/solution.py
@@ -39,8 +39,8 @@
 
 PARTS = 4
 PAD = 16
-CROSS = 9
-COPIES = CROSS + 25
+CROSS = 10
+COPIES = CROSS + 31
 
 
 def kernel(
@@ -53,7 +53,9 @@
     part = cols // PARTS
     hseq = seq // 2
     hrows = rows // 2
-    crows = rows * 9 // 32
+    hpart = part // 2
+    crows = rows * 6 // 32
+    zrows = rows // 8
     orest = hrows - crows
     count = taps_ref.shape[0]
     m = rep // 2
@@ -147,7 +149,7 @@
         local = {}
 
         def index(key):
-            if key[0] in ("tz", "gz", "oz"):
+            if key[0] in ("tz", "gz", "ge", "oz"):
                 return cross.setdefault(key, len(cross))
             return CROSS + local.setdefault(key, len(local))
 
@@ -171,11 +173,21 @@
                 device_id=to_t, device_id_type=MESH,
             ).wait_send()
 
-        chunks = PARTS - 1 if inside else 1
+        chunks = PARTS - 1 if inside else 2
         first = part if inside else 0
-        other_chunks = PARTS - chunks
-        other_first = 0 if inside else part
         units = 3 * chunks
+
+        def split(c):
+            return c == (0 if inside else 1)
+
+        def widths(c, act):
+            if not split(c):
+                act(0, part)
+                return
+            pl.when(tp == 0)(lambda: act(hpart if inside else 0, hpart))
+            if inside:
+                pl.when(tp == 1)(lambda: act(0, part))
+
         for u in range(units):
             c, w = u // 3, u % 3
             pltpu.make_async_copy(
@@ -188,8 +200,8 @@
             outw_hbm, outw.at[pl.ds(al(fs * rows, rows), rows)], local_sems.at[4])
         ow_load.start()
 
-        def wrow(u, f, off, n):
-            return wts.at[u, pl.ds(al(f * rows + off, 128), n)]
+        def wrow(u, f, off, n, lo, wd):
+            return wts.at[u, pl.ds(al(f * rows + off, 128), n), pl.ds(lo, wd)]
 
         def orow(f, off, n):
             return outw.at[pl.ds(al(f * rows + off, 16), n)]
@@ -208,38 +220,65 @@
         def tok_w(h):
             wait(("tt", h), tok.at[1, trow(h, 1 - tp)])
 
-        def gcols(t, base, c):
-            return pl.ds(al(t * cols + base + c * part, 128), part)
+        def gcols(c, lo, wd):
+            return pl.ds(al(tp * cols + first + c * part + lo, 128), wd)
 
         def grow(h):
             return pl.ds(0, seq) if h is None else pl.ds(h * hseq, hseq)
 
-        def z_key(c, h, from_inside):
-            return ("gz", c, h if from_inside and c == PARTS - 2 else None, from_inside)
-
         def own_gate(c, key):
             def store(r, x):
-                gat[r, gcols(tp, first, c)] = x
-            gate(c, first, 0, 0, 2, store)
-            here = gat.at[:, gcols(tp, first, c)]
-            send(key, here, here, to_t, 3)
+                def act(lo, wd):
+                    gat[r, gcols(c, lo, wd)] = x[:, lo : lo + wd]
+                widths(c, act)
+
+            def out(lo, wd):
+                here = gat.at[:, gcols(c, lo, wd)]
+                send(key, here, here, to_t, 3)
+
+            def run():
+                gate(c, first, 0, 0, 2, store)
+                widths(c, out)
+
+            if split(c) and not inside:
+                pl.when(tp == 0)(run)
+            else:
+                run()
 
         def partner_gate(c, h):
+            key = ("gz", c, h if c == PARTS - 2 else None) if inside else ("ge",)
+
             def store(r, x):
                 mine[c, r, :] = x
-            gate(c, first, 1, h or 0, 2 if h is None else 1, store)
-            send(z_key(c, h, inside), mine.at[c, grow(h)], gat.at[grow(h), gcols(tp, first, c)], to_z, 3)
-
-        def take(c, h, key):
-            here = gat.at[grow(h), gcols(tp, other_first, c)]
-            wait(z_key(c, h, not inside), here)
-            send(key, here, here, to_t, 3)
+
+            def out(lo, wd):
+                src = mine.at[c, grow(h), pl.ds(lo, wd)]
+                send(key, src, gat.at[grow(h), gcols(c, lo, wd)], to_z, 3)
+
+            def run():
+                gate(c, first, 1, h or 0, 2 if h is None else 1, store)
+                widths(c, out)
+
+            if split(c) and not inside:
+                pl.when(tp == 0)(run)
+            else:
+                run()
+
+        def forward(key, h, at, wd, new):
+            here = gat.at[grow(h), pl.ds(al(tp * cols + at, 128), wd)]
+            wait(key, here)
+            send(new, here, here, to_t, 3)
 
         def take_other(key, h, parts):
             wait(key, gat.at[grow(h), pl.ds(0, parts * part)])
 
         f_off, g_off = m * hrows, (1 - m) * hrows
         c_off, o_off = g_off + (1 - m) * orest, g_off + m * crows
+        zp_off, zq_off = g_off + m * (hrows - zrows), f_off + (1 - m) * (hrows - zrows)
+
+        def krow(f, off):
+            return al(f * rows + off, 128), hrows
+
 
         if inside:
             pl.semaphore_signal(barrier, inc=1, device_id=to_m, device_id_type=MESH)
@@ -248,22 +287,31 @@
 
             def direct(u):
                 c, w = u // 3, u % 3
-                at = pl.ds(first + c * part, part)
-                send(("d", u), hbm[w].at[pl.ds(al(hx, 128), hrows), at], wrow(u, fs, hx, hrows), to_x, 0)
-                send(("d", u), hbm[w].at[pl.ds(al(hy, 128), hrows), at], wrow(u, fs, hy, hrows), to_y, 0)
+
+                def act(lo, wd):
+                    at = pl.ds(first + c * part + lo, wd)
+                    for off, to in ((hx, to_x), (hy, to_y)):
+                        src = hbm[w].at[pl.ds(al(off, 128), hrows), at]
+                        send(("d", u), src, wrow(u, fs, off, hrows, lo, wd), to, 0)
+                widths(c, act)
 
             def relay(u):
-                wait(("d", u), wts.at[u, 0 : 2 * hrows])
-                bx, by = wrow(u, fx, hx, hrows), wrow(u, fy, hy, hrows)
-                send(("r", u), bx, bx, to_m, 0)
-                send(("r", u), by, by, to_x, 0)
-                send(("r", u), bx, bx, to_y, 0)
-                send(("r", u), by, by, to_m, 0)
+                def act(lo, wd):
+                    wait(("d", u), wts.at[u, 0 : 2 * hrows, lo : lo + wd])
+                    bx, by = wrow(u, fx, hx, hrows, lo, wd), wrow(u, fy, hy, hrows, lo, wd)
+                    send(("r", u), bx, bx, to_m, 0)
+                    send(("r", u), by, by, to_x, 0)
+                    send(("r", u), bx, bx, to_y, 0)
+                    send(("r", u), by, by, to_m, 0)
+                widths(u // 3, act)
 
             def ready(u):
                 if u == 0:
                     w_load.wait()
-                wait(("r", u), wts.at[u, 0 : 4 * hrows])
+                widths(u // 3, lambda lo, wd: wait(("r", u), wts.at[u, 0 : 4 * hrows, lo : lo + wd]))
+
+            def out_rows(key, off, n, to):
+                send(key, outw_hbm.at[pl.ds(al(off, 16), n)], orow(fs, off, n), to, 2)
 
             tok_z(0)
             tok_z(1)
@@ -282,6 +330,8 @@
             project([0], [0, 1])
             relay(3)
             direct(6)
+            out_rows(("oe",), zp_off, zrows, to_p)
+            out_rows(("oe",), zq_off, zrows, to_q)
             ready(1)
             project([1], [0, 1])
             tok_f(0)
@@ -300,19 +350,23 @@
             ready(3)
             project([3], [0, 1, 2])
             relay(6)
+            wait(("oe",), outw.at[0 : 2 * zrows])
+            for f, off in ((fp, zp_off), (fq, zq_off)):
+                block = orow(f, off, zrows)
+                send(("oz", 2), block, block, to_z, 2)
             ready(4)
+            tok_f(1)
             project([4], [0, 1, 2])
-            tok_f(1)
             relay(7)
             tok_w(1)
             norm(1, 1, 1)
             project([0, 1, 2], [3])
             partner_gate(0, 1)
             relay(8)
-            for b, (off, n) in enumerate(((f_off, hrows), (o_off, orest))):
-                src = outw_hbm.at[pl.ds(al(off, 16), n)]
-                send(("o", b), src, orow(fs, off, n), to_x, 2)
-                send(("o", b), src, orow(fs, off, n), to_y, 2)
+            out_rows(("o", 0), f_off, hrows, to_p)
+            out_rows(("o", 0), f_off + m * zrows, hrows - zrows, to_q)
+            out_rows(("o", 1), o_off + (1 - m) * zrows, orest - zrows, to_p)
+            out_rows(("o", 1), o_off, orest, to_q)
             ready(5)
             project([5], [0, 1, 2])
             partner_gate(1, 0)
@@ -338,56 +392,68 @@
             pl.when(tp == 1)(swap)
             project([8], [0, 1])
             own_gate(2, ("ga",))
-            take(0, None, ("ga",))
+            pl.when(tp == 0)(lambda: forward(("ge",), None, 0, part + hpart, ("ga",)))
+            pl.when(tp == 1)(lambda: forward(("ge",), None, 0, part, ("ga",)))
             ow_load.wait()
             take_other(("ga",), None, PARTS)
-            def krow(f, off):
-                return al(f * rows + off, 128), hrows
-
             mix(None, [(al(fs * rows, rows), rows), krow(fd, f_off)], True, False)
-            wait(("o", 0), outw.at[0 : 2 * hrows])
+            wait(("o", 0), outw.at[0 : 2 * hrows - zrows])
             mix(None, [krow(fx, f_off), krow(fy, f_off)], False, False)
             wait(("om",), orow(fd, g_off, hrows))
             mix(None, [krow(fd, g_off)], False, False)
             wait(("oz", 1), outw.at[0 : 2 * crows])
-            wait(("o", 1), outw.at[0 : 2 * orest])
+            wait(("o", 1), outw.at[0 : 2 * orest - zrows])
             mix(None, [krow(fx, g_off), krow(fy, g_off)], False, True)
-            wait_sent(0, wts.at[:, 0 : 6 * hrows])
+            pl.when(tp == 0)(lambda: wait_sent(0, wts.at[:, 0 : 5 * hrows]))
+            pl.when(tp == 1)(lambda: wait_sent(0, wts.at[:, 0 : 6 * hrows]))
             wait_sent(1, tok.at[0])
-            wait_sent(2, outw.at[0 : 3 * hrows + 2 * orest])
-            wait_sent(3, gat.at[:, 0 : 7 * part])
+            wait_sent(2, outw.at[0 : 3 * hrows + 2 * orest + 2 * zrows])
+            pl.when(tp == 0)(lambda: wait_sent(3, gat.at[:, 0 : 13 * hpart]))
+            pl.when(tp == 1)(lambda: wait_sent(3, gat.at[:, 0 : 14 * hpart]))
         else:
             pl.semaphore_wait(barrier, 4)
 
             def direct(u, which):
                 c, w = u // 3, u % 3
-                src = hbm[w].at[:, pl.ds(first + c * part, part)]
-                send(("d" + which, u), src, wrow(u, fs, 0, rows), to_p if which == "p" else to_q, 0)
+                wd = hpart if split(c) else part
+                src = hbm[w].at[:, pl.ds(first + c * part, wd)]
+                send(("d" + which, u), src, wrow(u, fs, 0, rows, 0, wd), to_p if which == "p" else to_q, 0)
 
             def relay_q(u):
-                wait(("dp", u), wrow(u, fp, 0, rows))
-                block = wrow(u, fp, f_off, hrows)
+                wd = hpart if split(u // 3) else part
+                wait(("dp", u), wrow(u, fp, 0, rows, 0, wd))
+                block = wrow(u, fp, f_off, hrows, 0, wd)
                 send(("r", u), block, block, to_q, 0)
 
             def relay_p(u):
-                wait(("dq", u), wrow(u, fq, 0, rows))
-                block = wrow(u, fq, g_off, hrows)
+                wd = hpart if split(u // 3) else part
+                wait(("dq", u), wrow(u, fq, 0, rows, 0, wd))
+                block = wrow(u, fq, g_off, hrows, 0, wd)
                 send(("r", u), block, block, to_p, 0)
 
             def ready(u):
                 if u == 0:
                     w_load.wait()
-                wait(("r", u), wts.at[u, 0 : 2 * hrows])
-
-            def out_rows(off):
-                return outw_hbm.at[pl.ds(al(off, 16), hrows)]
+                wd = hpart if split(u // 3) else part
+                wait(("r", u), wts.at[u, 0 : 2 * hrows, 0:wd])
+
+            def out_rows(key, off, n, to):
+                send(key, outw_hbm.at[pl.ds(al(off, 16), n)], orow(fs, off, n), to, 2)
+
+            extra = pl.when(tp == 0)
 
             tok_z(0)
             tok_z(1)
-            send(("op", 0), out_rows(f_off), orow(fs, f_off, hrows), to_p, 2)
+            out_rows(("op", 0), f_off, hrows, to_p)
             for u in range(3):
                 direct(u, "q")
                 direct(u, "p")
+
+            @extra
+            def _():
+                for u in range(3, 6):
+                    direct(u, "p")
+
             tok_load.wait()
             gain_load.wait()
             norm(0, 0, 2)
@@ -396,58 +462,96 @@
             block = orow(fp, f_off, hrows)
             wait(("op", 0), block)
             send(("orq",), block, block, to_q, 2)
+
+            @extra
+            def _():
+                for u in range(3, 6):
+                    direct(u, "q")
+
+
             relay_p(2)
-            send(("op", 1), out_rows(g_off), orow(fs, g_off, hrows), to_p, 2)
             relay_q(0)
             tok_f(0)
             relay_q(1)
             tok_w(0)
             norm(1, 0, 1)
             relay_q(2)
-            send(("oq", 0), out_rows(g_off), orow(fs, g_off, hrows), to_q, 2)
-            send(("oq", 1), out_rows(f_off), orow(fs, f_off, hrows), to_q, 2)
             block = orow(fd, f_off, hrows)
             wait(("orq",), block)
             send(("oz", 0), block, block, to_z, 2)
-            for u in range(2):
-                ready(u)
-                project([u], [0, 1, 2])
+
             tok_f(1)
-            ready(2)
-            project([2], [2])
-            taps_load.wait()
+            ready(0)
+            project([0], [0, 1, 2])
+
+            @extra
+            def _():
+                for u in range(3, 6):
+                    relay_p(u)
+                    relay_q(u)
+
+            ready(1)
+            project([1], [0, 1, 2])
+            out_rows(("op", 1), g_off + (1 - m) * zrows, hrows - zrows, to_p)
+            for b in range(2):
+                out_rows(("oq", b), g_off + b * hrows // 2, hrows // 2, to_q)
+            out_rows(("oq", 2), f_off + m * zrows, hrows - zrows, to_q)
             tok_w(1)
             norm(1, 1, 1)
+            ready(2)
+            taps_load.wait()
+            project([2], [2])
             project([0, 1, 2], [3])
             partner_gate(0, None)
+
+            @extra
+            def _():
+                for u in range(3, 6):
+                    ready(u)
+                project([3, 4, 5], [2, 3])
+            partner_gate(1, None)
+            def pass_on(b):
+                block = orow(fq, g_off + b * hrows // 2, hrows // 2)
+                wait(("oq", b), block)
+                send(("orp",), block, block, to_p, 2)
+
             project([2], [0, 1])
             own_gate(0, ("ga",))
-            wait(("op", 1), orow(fp, g_off, hrows))
+            pass_on(0)
+            extra(lambda: project([3, 4], [0, 1]))
+            wait(("op", 1), orow(fp, g_off, hrows - zrows))
             block = orow(fp, c_off, crows)
             send(("oz", 1), block, block, to_z, 4)
-            block = orow(fq, g_off, hrows)
-            wait(("oq", 0), block)
-            send(("orp",), block, block, to_p, 2)
+            extra(lambda: project([5], [0, 1]))
+            own_gate(1, ("ga",))
+            pl.when(tp == 0)(lambda: forward(("gz", 0, None), None, part + hpart, hpart, ("ga",)))
+            pl.when(tp == 1)(lambda: forward(("gz", 0, None), None, part, part, ("ga",)))
+            pass_on(1)
             block = orow(fq, c_off, crows)
             send(("oz", 1), block, block, to_z, 4)
-            take(0, None, ("ga",))
-            wait(("oq", 1), orow(fq, f_off, hrows))
+            forward(("gz", 1, None), None, 2 * part, part, ("gb",))
             ow_load.wait()
             take_other(("ga",), None, 2)
-            take(1, None, ("gb",))
-            wait(("orp",), orow(fd, g_off, hrows))
-            mix(None, [(0, 2 * part), (cols, 2 * part)], True, False)
             take_other(("gb",), None, 1)
-            mix(None, [(2 * part, part), (cols + 2 * part, part)], False, False)
+            wait(("oz", 2), outw.at[0 : 2 * zrows])
+            odd = lax.rem(fs, 2)
+            mix(None, [krow(fs, 0), krow(fp, 0), krow(fd + m * (fq - fd), 0),
+                       krow(fs + odd * (fx - fs), hrows)], True, False)
             for h in range(2):
-                take(2, h, ("gc", h))
+                forward(("gz", 2, h), h, 3 * part, part, ("gc", h))
+            wait(("oq", 2), orow(fq, f_off, hrows - zrows))
             for h in range(2):
                 take_other(("gc", h), h, 1)
-                mix(h, [(3 * part, part), (cols + 3 * part, part)], False, True)
-            wait_sent(0, wts.at[0:units, 0 : 6 * hrows])
+                mix(h, [krow(fq, f_off), krow(fp + m * (fd - fp), hrows),
+                        krow(fx + odd * (fs - fx), hrows)], False, False)
+            wait(("orp",), orow(fd, g_off, hrows))
+            mix(None, [krow(fd, g_off)], False, True)
+            pl.when(tp == 0)(lambda: wait_sent(0, wts.at[0:6, 0 : 9 * hrows // 2]))
+            pl.when(tp == 1)(lambda: wait_sent(0, wts.at[0:3, 0 : 6 * hrows]))
             wait_sent(1, tok.at[0])
-            wait_sent(2, outw.at[0 : 7 * hrows])
-            wait_sent(3, gat.at[:, 0 : 5 * part])
+            wait_sent(2, outw.at[0 : 7 * hrows - 2 * zrows])
+            pl.when(tp == 0)(lambda: wait_sent(3, gat.at[:, 0 : 11 * hpart]))
+            pl.when(tp == 1)(lambda: wait_sent(3, gat.at[:, 0 : 10 * hpart]))
             wait_sent(4, outw.at[0 : 2 * crows])
 
     @pl.when(inner_chip == 1)

time: 73.5 us -> 72.5 us (0.986); the launches traced: 73.3 us -> 71.2 us
  Pallas kernels: 72.2 us -> 70 us
    pallas_call x1, Pallas kernels: 72.2 us -> 70 us  [paired(): pl.pallas_call(kernel, out_shape=pltpu.VMEM((seq, cols), BF16), in_specs=...]
where the time goes in v4:
time: 72.5 us; the launch traced here: 71.2 us
  Pallas kernels  70 us (97%)
  local copies, waits for them, and re-layouts  1.15 us (2%)
    pallas_call x1, Pallas kernels, paired(): pl.pallas_call(kernel, out_shape=pltpu.VMEM((seq, cols), BF16), in_specs=...  70 us

profile of v4, /device:TPU:9, one launch (start us, length us, event | category | flops | bytes accessed | tf_op | source)
XLA Modules:
  0.0 71.2 jit_solution(15080405274538024244)
XLA Ops:
  0.0 70.0 %mixer.1 = bf16[768,1024]{1,0:T(8,128)(2,1)S(1)} custom-call(bf16[768,2048]{1,0:T(8,128)(2,1)} %bitcast.4, f32[1,2048]{1,0:T(1,128)} %bitcast.5, bf16[512,1024]{1,0:T(8,128)(2,1)} %outer_hbm.1, bf16[512,1024]{1,0:T(8,128)(2,1)} %inner_hbm.1, bf16[512,1024]{1,0:T(8,128)(2,1)} %value_hbm.1, f32[3,2048]{1,0:T(4,128)} %taps_hbm.1, bf16[512,1024]{1,0:T(8,128)(2,1)} %outw_hbm.1), custom_call_target="tpu_custom_call" | custom-call | tf_op jit(solution)/shard_map/mixer/pallas_call | solution.py:574
  70.0 1.1 %copy.9 = bf16[1,768,1024]{2,1,0:T(8,128)(2,1)} copy(bf16[1,768,1024]{2,1,0:T(8,128)(2,1)S(1)} %bitcast.3) | data formatting | bytes 3145728

commit v5 on v4

--- a/solution.py
+++ b/solution.py
@@ -495,7 +495,10 @@
             out_rows(("op", 1), g_off + (1 - m) * zrows, hrows - zrows, to_p)
             for b in range(2):
                 out_rows(("oq", b), g_off + b * hrows // 2, hrows // 2, to_q)
-            out_rows(("oq", 2), f_off + m * zrows, hrows - zrows, to_q)
+            def last_rows():
+                out_rows(("oq", 2), f_off + m * zrows, hrows - zrows, to_q)
+
+            extra(last_rows)
             tok_w(1)
             norm(1, 1, 1)
             ready(2)
@@ -527,6 +530,7 @@
             pl.when(tp == 0)(lambda: forward(("gz", 0, None), None, part + hpart, hpart, ("ga",)))
             pl.when(tp == 1)(lambda: forward(("gz", 0, None), None, part, part, ("ga",)))
             pass_on(1)
+            pl.when(tp == 1)(last_rows)
             block = orow(fq, c_off, crows)
             send(("oz", 1), block, block, to_z, 4)
             forward(("gz", 1, None), None, 2 * part, part, ("gb",))
@@ -540,12 +544,13 @@
             for h in range(2):
                 forward(("gz", 2, h), h, 3 * part, part, ("gc", h))
             wait(("oq", 2), orow(fq, f_off, hrows - zrows))
-            for h in range(2):
-                take_other(("gc", h), h, 1)
-                mix(h, [krow(fq, f_off), krow(fp + m * (fd - fp), hrows),
-                        krow(fx + odd * (fs - fx), hrows)], False, False)
+            late = [krow(fq, f_off), krow(fp + m * (fd - fp), hrows), krow(fx + odd * (fs - fx), hrows)]
+            take_other(("gc", 0), 0, 1)
+            mix(0, late, False, False)
             wait(("orp",), orow(fd, g_off, hrows))
-            mix(None, [krow(fd, g_off)], False, True)
+            mix(0, [krow(fd, g_off)], False, True)
+            take_other(("gc", 1), 1, 1)
+            mix(1, late + [krow(fd, g_off)], False, True)
             pl.when(tp == 0)(lambda: wait_sent(0, wts.at[0:6, 0 : 9 * hrows // 2]))
             pl.when(tp == 1)(lambda: wait_sent(0, wts.at[0:3, 0 : 6 * hrows]))
             wait_sent(1, tok.at[0])

time: 72.5 us -> 71.8 us (level)
  no operation moved by 1% of the time
where the time goes in v5:
time: 71.8 us; the launch traced here: 71.2 us
  Pallas kernels  70 us (97%)
  local copies, waits for them, and re-layouts  1.15 us (2%)
    pallas_call x1, Pallas kernels, paired(): pl.pallas_call(kernel, out_shape=pltpu.VMEM((seq, cols), BF16), in_specs=...  70 us

profile of v5, /device:TPU:9, one launch (start us, length us, event | category | flops | bytes accessed | tf_op | source)
XLA Modules:
  0.0 71.2 jit_solution(8362926676876608511)
XLA Ops:
  0.0 70.0 %mixer.1 = bf16[768,1024]{1,0:T(8,128)(2,1)S(1)} custom-call(bf16[768,2048]{1,0:T(8,128)(2,1)} %bitcast.4, f32[1,2048]{1,0:T(1,128)} %bitcast.5, bf16[512,1024]{1,0:T(8,128)(2,1)} %outer_hbm.1, bf16[512,1024]{1,0:T(8,128)(2,1)} %inner_hbm.1, bf16[512,1024]{1,0:T(8,128)(2,1)} %value_hbm.1, f32[3,2048]{1,0:T(4,128)} %taps_hbm.1, bf16[512,1024]{1,0:T(8,128)(2,1)} %outw_hbm.1), custom_call_target="tpu_custom_call" | custom-call | tf_op jit(solution)/shard_map/mixer/pallas_call | solution.py:579
  70.0 1.1 %copy.9 = bf16[1,768,1024]{2,1,0:T(8,128)(2,1)} copy(bf16[1,768,1024]{2,1,0:T(8,128)(2,1)S(1)} %bitcast.3) | data formatting | bytes 3145728

commit v6 on v5

--- a/solution.py
+++ b/solution.py
@@ -40,7 +40,7 @@
 PARTS = 4
 PAD = 16
 CROSS = 10
-COPIES = CROSS + 31
+COPIES = CROSS + 25
 
 
 def kernel(
@@ -417,19 +417,21 @@
                 c, w = u // 3, u % 3
                 wd = hpart if split(c) else part
                 src = hbm[w].at[:, pl.ds(first + c * part, wd)]
-                send(("d" + which, u), src, wrow(u, fs, 0, rows, 0, wd), to_p if which == "p" else to_q, 0)
+                send(("d" + which, min(u, 3)), src, wrow(u, fs, 0, rows, 0, wd), to_p if which == "p" else to_q, 0)
 
             def relay_q(u):
                 wd = hpart if split(u // 3) else part
-                wait(("dp", u), wrow(u, fp, 0, rows, 0, wd))
+                if u < 3:
+                    wait(("dp", u), wrow(u, fp, 0, rows, 0, wd))
                 block = wrow(u, fp, f_off, hrows, 0, wd)
-                send(("r", u), block, block, to_q, 0)
+                send(("r", min(u, 3)), block, block, to_q, 0)
 
             def relay_p(u):
                 wd = hpart if split(u // 3) else part
-                wait(("dq", u), wrow(u, fq, 0, rows, 0, wd))
+                if u < 3:
+                    wait(("dq", u), wrow(u, fq, 0, rows, 0, wd))
                 block = wrow(u, fq, g_off, hrows, 0, wd)
-                send(("r", u), block, block, to_p, 0)
+                send(("r", min(u, 3)), block, block, to_p, 0)
 
             def ready(u):
                 if u == 0:
@@ -486,6 +488,8 @@
 
             @extra
             def _():
+                wait(("dq", 3), wts.at[3:6, 0:rows, 0:hpart])
+                wait(("dp", 3), wts.at[3:6, 0:rows, 0:hpart])
                 for u in range(3, 6):
                     relay_p(u)
                     relay_q(u)
@@ -509,8 +513,7 @@
 
             @extra
             def _():
-                for u in range(3, 6):
-                    ready(u)
+                wait(("r", 3), wts.at[3:6, 0 : 2 * hrows, 0:hpart])
                 project([3, 4, 5], [2, 3])
             partner_gate(1, None)
             def pass_on(b):

time: 71.8 us -> 71.8 us (level)
  no operation moved by 1% of the time
where the time goes in v6:
time: 71.8 us; the launch traced here: 71.1 us
  Pallas kernels  70 us (97%)
  local copies, waits for them, and re-layouts  1.15 us (2%)
    pallas_call x1, Pallas kernels, paired(): pl.pallas_call(kernel, out_shape=pltpu.VMEM((seq, cols), BF16), in_specs=...  70 us

profile of v6, /device:TPU:9, one launch (start us, length us, event | category | flops | bytes accessed | tf_op | source)
XLA Modules:
  0.0 71.1 jit_solution(16979556639557929348)
XLA Ops:
  0.0 70.0 %mixer.1 = bf16[768,1024]{1,0:T(8,128)(2,1)S(1)} custom-call(bf16[768,2048]{1,0:T(8,128)(2,1)} %bitcast.4, f32[1,2048]{1,0:T(1,128)} %bitcast.5, bf16[512,1024]{1,0:T(8,128)(2,1)} %outer_hbm.1, bf16[512,1024]{1,0:T(8,128)(2,1)} %inner_hbm.1, bf16[512,1024]{1,0:T(8,128)(2,1)} %value_hbm.1, f32[3,2048]{1,0:T(4,128)} %taps_hbm.1, bf16[512,1024]{1,0:T(8,128)(2,1)} %outw_hbm.1), custom_call_target="tpu_custom_call" | custom-call | tf_op jit(solution)/shard_map/mixer/pallas_call | solution.py:582
  70.0 1.1 %copy.9 = bf16[1,768,1024]{2,1,0:T(8,128)(2,1)} copy(bf16[1,768,1024]{2,1,0:T(8,128)(2,1)S(1)} %bitcast.3) | data formatting | bytes 3145728
